TPU v7x, 256 devices: a whole 4x4x8 slice. The times are simulated.
256 devices in a mesh: sp: 16 (over y, x), tp: 16 (over z, core).
Axes of the slice: x: 4, y: 4, z: 8, core: 2. Of those that a mesh axis runs over, the one named last changes fastest.
Arguments:
- tokens: bfloat16 [8192, 2048], P(('sp', 'tp')), may hold values from -6 to 6
- query_vectors: bfloat16 [8192, 2048], P('sp', 'tp'), may hold values from -8 to 8
- key_vectors: bfloat16 [8192, 2048], P('sp', 'tp'), may hold values from -8 to 8
- value_vectors: bfloat16 [8192, 2048], P('sp', 'tp'), may hold values from -24 to 24
- cum_gate: float32 [8192, 32], P('sp', 'tp'), may hold values from -1028 to 0, as said below
- out_weight: bfloat16 [2048, 2048], P('tp'), may hold values from -0.125 to 0.125
- norm_gain: float32 [2048], replicated, may hold values from 0.1 to 1.9
- gate_weight: bfloat16 [16, 2048, 7168], P('sp', None, 'tp'), may hold values from -0.125 to 0.125
- up_weight: bfloat16 [16, 2048, 7168], P('sp', None, 'tp'), may hold values from -0.125 to 0.125
- down_weight: bfloat16 [16, 7168, 2048], P('sp', 'tp'), may hold values from -0.0625 to 0.0625
- expert_ids: int32 [8192, 2], P(('sp', 'tp')), may hold values from 0 to 15, all different within a row; in each aligned block of 32 rows (0 to 31, 32 to 63, ...) at most 6 rows name the same one
- route_weights: float32 [8192, 2], P(('sp', 'tp')), may hold values from 0.2 to 1
Outputs:
- layer_output: bfloat16 [8192, 2048], P(('sp', 'tp'))
Inputs may be any that keep to these rules, and one draw needn't show every extreme that they name: `cum_gate`: along the positions each head's values never rise. `expert_ids`: within the rows of one device no expert is named by more than 6 rows, and in some devices' rows one expert is named by exactly 6; a row names 2 different experts.
All inputs are finite; a program needn't handle non-finite values.
Results may differ from a plain program's by a relative error of at most 0.014.
Values may be sent and summed in bfloat16 or wider, within the bound.
A program may use at most 128 MiB of HBM per device.

v0:
```python
import math
import jax
import jax.numpy as jnp
from jax import lax
from jax.sharding import PartitionSpec as P

NEG_LARGE = -1e30


def copy_for_each(shard, axis):
    peers = lax.axis_size(axis)
    return lax.all_to_all(
        jnp.broadcast_to(shard[None], (peers, *shard.shape)), axis, 0, 0, tiled=True
    )


def in_order(parts, dim):
    parts = jnp.moveaxis(parts, 0, dim)
    dims = parts.shape
    return parts.reshape(*dims[:dim], dims[dim] * dims[dim + 1], *dims[dim + 2 :])


def collect(shard, axis, dim):
    parts = copy_for_each(shard, axis)
    return in_order(parts, dim)


def sent_together(arrays, axis, dim, along):
    widths = [a.shape[along] for a in arrays]
    both = jnp.concatenate(arrays, axis=along)
    filled = lax.all_gather(both, axis, axis=dim, tiled=True)
    return tuple(jnp.split(filled, [sum(widths[:k]) for k in range(1, len(widths))], axis=along))


def shards(
    tokens,
    query_vectors,
    key_vectors,
    value_vectors,
    cum_gate,
    out_weight,
    norm_gain,
    gate_weight,
    up_weight,
    down_weight,
    expert_ids,
    route_weights,
):
    sp_count = lax.axis_size("sp")
    seg_rows = query_vectors.shape[0]
    heads_here = cum_gate.shape[1]
    head_width = query_vectors.shape[1] // heads_here
    score_scale = head_width ** (-0.5)
    offset = lax.axis_index("sp") * seg_rows
    last_query = offset + seg_rows - 1
    query_pos = offset + jnp.arange(seg_rows, dtype=jnp.int32)
    query_heads = query_vectors.reshape(seg_rows, heads_here, head_width)
    query_gate = cum_gate.T
    gate_rows = collect(cum_gate, "sp", 0)

    def attend_block(carried, key_block, value_block, block_start):
        running_peak, running_total, accumulated = carried
        row_count = key_block.shape[0]
        key_heads = key_block.reshape(row_count, heads_here, head_width)
        value_heads = value_block.reshape(row_count, heads_here, head_width)
        key_gate = lax.dynamic_slice_in_dim(gate_rows, block_start, row_count, 0).T
        scores = (
            jnp.einsum("qhd,khd->hqk", query_heads, key_heads, preferred_element_type=jnp.float32)
            * score_scale
        )
        scores = scores + query_gate[:, :, None] - key_gate[:, None, :]
        key_pos = block_start + jnp.arange(row_count, dtype=jnp.int32)
        visible = (key_pos[None, :] <= query_pos[:, None])[None]
        scores = jnp.where(visible, scores, NEG_LARGE)
        new_peak = jnp.maximum(running_peak, jnp.max(scores, axis=2))
        exponent = jnp.where(visible, jnp.exp(scores - new_peak[:, :, None]), 0.0)
        rescale = jnp.exp(running_peak - new_peak)
        running_total = running_total * rescale + jnp.sum(exponent, axis=2)
        weighted = jnp.einsum(
            "hqk,khd->hqd",
            exponent.astype(jnp.bfloat16),
            value_heads,
            preferred_element_type=jnp.float32,
        )
        accumulated = accumulated * rescale[:, :, None] + weighted
        return (new_peak, running_total, accumulated)

    start_state = (
        jnp.full((heads_here, seg_rows), NEG_LARGE, jnp.float32),
        jnp.zeros((heads_here, seg_rows), jnp.float32),
        jnp.zeros((heads_here, seg_rows, head_width), jnp.float32),
    )
    carried = start_state
    key_piece, value_piece = sent_together((key_vectors, value_vectors), "sp", 0, 1)
    row_count = key_piece.shape[0]
    block_rows = math.gcd(row_count, 1024)
    block_count = row_count // block_rows
    key_stack = key_piece.reshape(block_count, block_rows, key_piece.shape[1])
    value_stack = value_piece.reshape(block_count, block_rows, value_piece.shape[1])

    def step_block(state, inputs):
        key_block, value_block, block_index = inputs
        block_start = block_index * block_rows

        def take_block(inner):
            return attend_block(inner, key_block, value_block, block_start)

        def skip_block(inner):
            return inner

        return (lax.cond(block_start <= last_query, take_block, skip_block, state), None)

    carried, _ = lax.scan(
        step_block, carried, (key_stack, value_stack, jnp.arange(block_count, dtype=jnp.int32))
    )
    final_peak, final_total, accumulated = carried
    attended = (accumulated / final_total[:, :, None]).astype(jnp.bfloat16)
    attended = attended.transpose(1, 0, 2).reshape(seg_rows, heads_here * head_width)
    tok_dev = tokens.shape[0]
    model_width = tokens.shape[1]
    token_rows = lax.all_to_all(attended, "tp", split_axis=0, concat_axis=1, tiled=True)
    projected = jnp.dot(
        token_rows,
        lax.all_gather(out_weight, "tp", axis=0, tiled=True),
        preferred_element_type=jnp.float32,
    )
    stream_wide = (tokens.astype(jnp.float32) + projected).astype(jnp.bfloat16).astype(jnp.float32)
    inverse = lax.rsqrt(jnp.mean(stream_wide * stream_wide, axis=1, keepdims=True) + 1e-05)
    normed = (stream_wide * inverse * norm_gain[None, :]).astype(jnp.bfloat16)
    n_experts = gate_weight.shape[0] * sp_count
    top_count = expert_ids.shape[1]
    capacity = max(2, 3 * tok_dev * top_count // (2 * n_experts))
    flat_ids = expert_ids.reshape(-1)
    hits = (flat_ids[:, None] == jnp.arange(n_experts, dtype=jnp.int32)[None, :]).astype(jnp.int32)
    earlier = jnp.cumsum(hits, axis=0) - hits
    slot_index = flat_ids * capacity + jnp.sum(earlier * hits, axis=1)
    placement_map = (
        jnp.arange(n_experts * capacity, dtype=jnp.int32)[:, None] == slot_index[None, :]
    ).astype(jnp.bfloat16)
    repeated = jnp.repeat(normed, top_count, axis=0)
    dispatch = jnp.dot(placement_map, repeated, preferred_element_type=jnp.float32).astype(
        jnp.bfloat16
    )
    dispatch = dispatch.reshape(n_experts, capacity, model_width)
    arrived = lax.all_to_all(dispatch, "sp", split_axis=0, concat_axis=0, tiled=True)
    row_block = arrived.reshape(-1, model_width)
    rows_in = lax.all_gather(row_block, "tp", axis=0, tiled=True)
    gate_value = jnp.dot(rows_in, gate_weight[0], preferred_element_type=jnp.float32)
    up_value = jnp.dot(rows_in, up_weight[0], preferred_element_type=jnp.float32)
    hidden = (jax.nn.silu(gate_value) * up_value).astype(jnp.bfloat16)
    summed = lax.psum_scatter(
        jnp.dot(hidden, down_weight[0], preferred_element_type=jnp.float32).astype(jnp.bfloat16),
        "tp",
        scatter_dimension=0,
        tiled=True,
    )
    returned = summed.reshape(arrived.shape)
    back = lax.all_to_all(returned, "sp", split_axis=0, concat_axis=0, tiled=True)
    flat_back = back.reshape(n_experts * capacity, model_width)
    picked = flat_back[slot_index].astype(jnp.float32).reshape(tok_dev, top_count, model_width)
    mixture = jnp.sum(picked * route_weights[:, :, None], axis=1)
    return (stream_wide + mixture).astype(jnp.bfloat16)


def solution(mesh):
    in_specs = (
        P(("sp", "tp"), None),
        P("sp", "tp"),
        P("sp", "tp"),
        P("sp", "tp"),
        P("sp", "tp"),
        P("tp", None),
        P(),
        P("sp", None, "tp"),
        P("sp", None, "tp"),
        P("sp", "tp", None),
        P(("sp", "tp"), None),
        P(("sp", "tp"), None),
    )
    out_specs = P(("sp", "tp"), None)
    return jax.shard_map(shards, mesh=mesh, in_specs=in_specs, out_specs=out_specs, check_vma=False)
```

profile of v0, /device:TPU:2, one launch (start us, length us, event | category | flops | bytes accessed | tf_op | source)
XLA Modules:
  0.0 335.4 jit_solution(8175806650671181984)
XLA Ops:
  6.5 1.8 pad_maximum_fusion
  8.4 0.7 all-gather.6.cloned.1.call-update
  9.2 1.3 broadcast_in_dim.61
  10.5 7.5 %all-to-all-start = ((f32[16,512,2]{1,2,0:T(2,128)}), f32[16,512,2]{1,2,0:T(2,128)S(1)}, u32[]{:S(2)}, u32[]{:S(2)}) async-start(f32[16,512,2]{1,2,0:T(2,128)} %broadcast_in_dim.61), calls=%async_computation | async-start | bytes 131072 | tf_op jit(solution)/shard_map/all_to_all | solution.py:12
  18.0 1.0 copy.28
  19.0 0.8 copy.33
  20.0 49.1 %all-gather.4.cloned.1.call-done = bf16[8192,256]{1,0:T(8,128)(2,1)} async-done(((bf16[512,256]{1,0:T(8,128)(2,1)}), bf16[8192,256]{1,0:T(8,128)(2,1)}) %all-gather.4.cloned.1.call-update) | async-done | bytes 4194320 | tf_op jit(solution)/shard_map/all_gather | solution.py:31
  69.2 4.4 %fusion.30 = (bf16[8192,128]{1,0:T(8,128)(2,1)}, bf16[8192,128]{1,0:T(8,128)(2,1)}) fusion(bf16[8192,256]{1,0:T(8,128)(2,1)} %all-gather.4.cloned.1.call-done), kind=kLoop, calls=%fused_computation.54 | loop fusion | bytes 8388608 | tf_op jit(solution)/shard_map/split | solution.py:32
  73.6 3.9 %copy.29 = bf16[8,1024,128]{1,2,0:T(8,128)(2,1)} copy(bf16[8,1024,128]{2,1,0:T(8,128)(2,1)} %bitcast.60) | data formatting | bytes 4194304
  77.5 3.9 %copy.30 = bf16[8,1024,128]{1,2,0:T(8,128)(2,1)} copy(bf16[8,1024,128]{2,1,0:T(8,128)(2,1)} %bitcast.59) | data formatting | bytes 4194304
  81.5 16.5 %while.15 = (s32[]{:T(128)}, f32[2,512]{1,0:T(2,128)S(1)}, f32[2,512]{1,0:T(2,128)S(1)}, f32[2,512,64]{1,2,0:T(8,128)S(1)}, s32[8]{0:T(128)S(1)}, /*index=5*/s32...) while((s32[]{:T(128)}, f32[2,512]{1,0:T(2,128)S(1)}, ...), condition=%wide.region_5.6_spmd.clone, body=%wide.region_0.5_spmd.clone.sunk | while | flops 289017344 | bytes 17043828 | solution.py:113
  81.5 0.6 dynamic_slice.31
  82.8 6.2 %conditional.3 = ((f32[2,512]{1,0:T(2,128)S(1)}, f32[2,512]{1,0:T(2,128)S(1)}, f32[2,512,64]{1,2,0:T(8,128)S(1)})) conditional(s32[]{:T(128)} %convert_element_type.83, (f32[2,512]{1,0:T(2,128)S(1)}, f32[2,512]{1,0:T(2,128)S(1)}, f32[2,512,64]{1,2,0:T(8,128)S(1)}) %tuple.43, (s32[]{:T(128)}, s32[]{:T(128)}, bf16[8,1024,128]{1,2,0:T(8,128)(2,1)}, ...), branch_computations={%region_1.1_spmd, %region_2.4_spmd} | conditional | flops 289017344 | bytes 17041490 | solution.py:111
  82.9 0.4 broadcast_compare_fusion
  83.3 1.1 constant_dynamic-slice_fusion
  84.3 1.4 fusion.4
  85.7 1.5 fusion.3
  87.2 1.7 fusion.8
  89.0 0.6 dynamic_slice.31
  90.3 0.6 dynamic_slice.31
  91.6 0.6 dynamic_slice.31
  92.9 0.6 dynamic_slice.31
  94.2 0.6 dynamic_slice.31
  95.5 0.6 dynamic_slice.31
  96.7 0.6 dynamic_slice.31
  98.1 0.2 copy.31
  98.2 0.8 all_to_all.24
  99.0 7.1 %all-to-all-start.1 = ((bf16[16,32,128]{2,1,0:T(8,128)(2,1)}), bf16[16,32,128]{2,1,0:T(8,128)(2,1)S(1)}, u32[]{:S(2)}, u32[]{:S(2)}) async-start(bf16[16,32,128]{2,1,0:T(8,128)(2,1)} %all_to_all.24), calls=%async_computation.1 | async-start | bytes 262144 | tf_op jit(solution)/shard_map/all_to_all | solution.py:121
  106.2 0.2 select_reduce_fusion
  106.4 10.4 %all-to-all-done.1 = bf16[16,32,128]{2,1,0:T(8,128)(2,1)S(1)} async-done(((bf16[16,32,128]{2,1,0:T(8,128)(2,1)}), bf16[16,32,128]{2,1,0:T(8,128)(2,1)S(1)}, u32[]{:S(2)}, u32[]{:S(2)}) %all-to-all-start.1) | async-done | bytes 131104 | tf_op jit(solution)/shard_map/all_to_all | solution.py:121
  116.8 12.6 %all-gather.6.cloned.1.call-done = bf16[2048,2048]{1,0:T(8,128)(2,1)} async-done(((bf16[128,2048]{1,0:T(8,128)(2,1)}), bf16[2048,2048]{1,0:T(8,128)(2,1)}) %all-gather.6.cloned.1.call-update) | async-done | bytes 8388624 | tf_op jit(solution)/shard_map/all_gather | solution.py:124
  129.4 5.0 %multiply_reduce_fusion.1 = (f32[32]{0:T(128)S(1)}, f32[32,2048]{1,0:T(8,128)S(1)}) fusion(bf16[2048,2048]{1,0:T(8,128)(2,1)} %all-gather.6.cloned.1.call-done, bf16[32,2048]{1,0:T(8,128)(2,1)S(1)} %copy-done.2, bf16[16,32,128]{2,1,0:T(8,128)(2,1)S(1)} %all-to-all-done.1), kind=kOutput, calls=%fused_computation.36 | convolution fusion | flops 268828640 | bytes 8913024 | tf_op jit(solution)/shard_map/dot_general | solution.py:122
  134.6 0.1 broadcast_in_dim.62
  134.9 0.2 convolution_convert_fusion.1
  135.2 44.9 %all_to_all.34 = bf16[16,6,2048]{2,1,0:T(8,128)(2,1)S(1)} all-to-all(bf16[16,6,2048]{2,1,0:T(8,128)(2,1)S(1)} %reshape.145), channel_id=1, replica_groups=mesh['sp'=16,'tp'=16] {'sp'}, dimensions={0} | all-to-all | bytes 786432 | tf_op jit(solution)/shard_map/all_to_all | solution.py:145
  180.1 0.9 reshape.146
  181.1 0.2 reduce-scatter.2.cloned.1.call-start
  181.3 40.0 %all-gather.8.cloned.1.call-done = bf16[1536,2048]{1,0:T(8,128)(2,1)} async-done(((bf16[96,2048]{1,0:T(8,128)(2,1)}), bf16[1536,2048]{1,0:T(8,128)(2,1)}) %all-gather.8.cloned.1.call-update) | async-done | bytes 6291472 | tf_op jit(solution)/shard_map/all_gather | solution.py:147
  221.2 7.9 %fusion.19 = f32[1536,448]{0,1:T(8,128)} fusion(bf16[1536,2048]{1,0:T(8,128)(2,1)} %all-gather.8.cloned.1.call-done, bf16[1,2048,448]{1,2,0:T(8,128)(2,1)} %param.23), kind=kOutput, calls=%fused_computation.30 | convolution fusion | flops 2818572288 | bytes 10878976 | tf_op jit(solution)/shard_map/dot_general | solution.py:148
  229.1 13.2 %convolution_convert_fusion = bf16[1536,2048]{1,0:T(8,128)(2,1)} fusion(bf16[1,448,2048]{2,1,0:T(8,128)(2,1)S(1)} %copy-done, bf16[1536,2048]{1,0:T(8,128)(2,1)} %all-gather.8.cloned.1.call-done, f32[1536,448]{0,1:T(8,128)} %fusion.19, bf16[1,2048,448]{1,2,0:T(8,128)(2,1)} %param.24), kind=kOutput, calls=%fused_computation.21 | convolution fusion | flops 5644419072 | bytes 19005440 | tf_op jit(solution)/shard_map/dot_general | solution.py:152
  242.3 65.9 %reduce-scatter.2.cloned.1.call-done = bf16[96,2048]{1,0:T(8,128)(2,1)} async-done(((bf16[1536,2048]{1,0:T(8,128)(2,1)}), bf16[96,2048]{1,0:T(8,128)(2,1)}) %reduce-scatter.2.cloned.1.call-update) | async-done | bytes 393232 | tf_op jit(solution)/shard_map/reduce_scatter | solution.py:151
  308.2 1.9 reshape.147
  310.2 7.2 %all-to-all-start.3 = ((bf16[16,6,2048]{2,1,0:T(8,128)(2,1)}), bf16[16,6,2048]{2,1,0:T(8,128)(2,1)S(1)}, u32[]{:S(2)}, u32[]{:S(2)}) async-start(bf16[16,6,2048]{2,1,0:T(8,128)(2,1)} %reshape.147), calls=%async_computation.4 | async-start | bytes 1048576 | tf_op jit(solution)/shard_map/all_to_all | solution.py:158
  317.7 8.5 %all-to-all-done.3 = bf16[16,6,2048]{2,1,0:T(8,128)(2,1)S(1)} async-done(((bf16[16,6,2048]{2,1,0:T(8,128)(2,1)}), bf16[16,6,2048]{2,1,0:T(8,128)(2,1)S(1)}, u32[]{:S(2)}, u32[]{:S(2)}) %all-to-all-start.3) | async-done | bytes 393248 | tf_op jit(solution)/shard_map/all_to_all | solution.py:158
  326.3 0.7 gather_fusion
  327.1 0.3 reshape.149
  327.4 0.7 multiply_reduce_fusion
  328.1 0.7 add_convert_fusion
  (60 shorter events, 1.5 us)
Async XLA Ops:
  6.5 222.6 %copy-start = (bf16[1,448,2048]{2,1,0:T(8,128)(2,1)S(1)}, bf16[1,448,2048]{2,1,0:T(8,128)(2,1)}, u32[]{:S(2)}) copy-start(bf16[1,448,2048]{2,1,0:T(8,128)(2,1)} %param.25) | copy-start | bytes 5505028
  6.5 62.6 %all-gather.4.cloned.1.call-start = ((), (), s32[]{:S(2)}) async-start(), calls=%async_computation.5 | async-start | bytes 4456448 | tf_op jit(solution)/shard_map/all_gather | solution.py:31
  8.4 121.0 %all-gather.6.cloned.1.call-start = ((), (), s32[]{:S(2)}) async-start(), calls=%async_computation.6 | async-start | bytes 8912896 | tf_op jit(solution)/shard_map/all_gather | solution.py:124
  10.5 70.9 %all-to-all-start = ((f32[16,512,2]{1,2,0:T(2,128)}), f32[16,512,2]{1,2,0:T(2,128)S(1)}, u32[]{:S(2)}, u32[]{:S(2)}) async-start(f32[16,512,2]{1,2,0:T(2,128)} %broadcast_in_dim.61), calls=%async_computation | async-start | bytes 131072 | tf_op jit(solution)/shard_map/all_to_all | solution.py:12
  73.6 7.9 %copy-start.1 = (f32[512,2]{0,1:T(2,128)S(1)}, f32[512,2]{0,1:T(2,128)}, u32[]{:S(2)}) copy-start(f32[512,2]{0,1:T(2,128)} %param.20) | copy-start | bytes 12292
  81.5 47.9 %copy-start.2 = (bf16[32,2048]{1,0:T(8,128)(2,1)S(1)}, bf16[32,2048]{1,0:T(8,128)(2,1)}, u32[]{:S(2)}) copy-start(bf16[32,2048]{1,0:T(8,128)(2,1)} %param.16) | copy-start | bytes 393220
  99.0 17.7 %all-to-all-start.1 = ((bf16[16,32,128]{2,1,0:T(8,128)(2,1)}), bf16[16,32,128]{2,1,0:T(8,128)(2,1)S(1)}, u32[]{:S(2)}, u32[]{:S(2)}) async-start(bf16[16,32,128]{2,1,0:T(8,128)(2,1)} %all_to_all.24), calls=%async_computation.1 | async-start | bytes 262144 | tf_op jit(solution)/shard_map/all_to_all | solution.py:121
  106.1 115.1 %all-gather.8.cloned.1.call-start = ((), (), s32[]{:S(2)}) async-start(), calls=%async_computation.7 | async-start | bytes 6684672 | tf_op jit(solution)/shard_map/all_gather | solution.py:147
  106.4 28.1 %copy-start.3 = (f32[2048]{0:T(1024)S(1)}, f32[2048]{0:T(1024)}, u32[]{:S(2)}) copy-start(f32[2048]{0:T(1024)} %param.22) | copy-start | bytes 24580
  181.1 127.2 %reduce-scatter.2.cloned.1.call-start = ((), (), s32[]{:S(2)}) async-start(), calls=%async_computation.8 | async-start | bytes 6684672 | tf_op jit(solution)/shard_map/reduce_scatter | solution.py:151
  242.3 75.1 %copy-start.4 = (s32[32,2]{0,1:T(2,128)S(1)}, s32[32,2]{0,1:T(2,128)}, u32[]{:S(2)}) copy-start(s32[32,2]{0,1:T(2,128)} %param.26) | copy-start | bytes 772
  242.3 75.3 %copy-start.5 = (f32[32,2]{0,1:T(2,128)S(1)}, f32[32,2]{0,1:T(2,128)}, u32[]{:S(2)}) copy-start(f32[32,2]{0,1:T(2,128)} %param.27) | copy-start | bytes 772
  310.2 16.0 %all-to-all-start.3 = ((bf16[16,6,2048]{2,1,0:T(8,128)(2,1)}), bf16[16,6,2048]{2,1,0:T(8,128)(2,1)S(1)}, u32[]{:S(2)}, u32[]{:S(2)}) async-start(bf16[16,6,2048]{2,1,0:T(8,128)(2,1)} %reshape.147), calls=%async_computation.4 | async-start | bytes 1048576 | tf_op jit(solution)/shard_map/all_to_all | solution.py:158
Sparse Core Ops, SparseCore 0:
  9.8 59.3 all-gather.3
  71.0 58.3 all-gather.5
  181.2 40.0 all-gather.7
  242.5 65.7 reduce-scatter.1
where the time goes:
time: 336 us; the launch traced here: 335 us
  waiting for transfers between devices  187 us (56%)
  blocking collectives  44.9 us (13%)
  matrix products  29.4 us (9%)
  local copies, waits for them, and re-layouts  27.1 us (8%)
  starting transfers between devices  22.1 us (7%)
  between operations  13.3 us (4%)
  loops' own time  5.68 us (2%)
  other arithmetic  5.62 us (2%)
    reduce_scatter x1, waiting for transfers between devices, shards(): lax.psum_scatter(jnp.dot(hidden, down_weight[0], preferred_element_type=j...  65.9 us
    all_gather x1, waiting for transfers between devices, sent_together(): filled = lax.all_gather(both, axis, axis=dim, tiled=True)  49.1 us
    all_to_all x1, blocking collectives, shards(): lax.all_to_all(dispatch, 'sp', split_axis=0, concat_axis=0, tiled=True)  44.9 us
    all_gather x1, waiting for transfers between devices, shards(): rows_in = lax.all_gather(row_block, 'tp', axis=0, tiled=True)  40 us
    dot_general x1, matrix products, shards(): jnp.dot(hidden, down_weight[0], preferred_element_type=jnp.float32)  13.2 us
    all_gather x1, waiting for transfers between devices, shards(): lax.all_gather(out_weight, 'tp', axis=0, tiled=True)  12.6 us
    all_to_all x1, waiting for transfers between devices, shards(): lax.all_to_all(attended, 'tp', split_axis=0, concat_axis=1, tiled=True)  10.4 us
    unnamed x17, local copies, waits for them, and re-layouts  9.73 us
  transfers between devices with their start and end apart: 7, of which 6 were waited for; matrix products, arithmetic and copies ran while one was open for 8% of the time, Pallas kernels for 0%

commit v1 on v0

--- a/solution.py
+++ b/solution.py
@@ -144,7 +144,34 @@
     dispatch = dispatch.reshape(n_experts, capacity, model_width)
     arrived = lax.all_to_all(dispatch, "sp", split_axis=0, concat_axis=0, tiled=True)
     row_block = arrived.reshape(-1, model_width)
-    rows_in = lax.all_gather(row_block, "tp", axis=0, tiled=True)
+
+    def threads_lay(payload):
+        then, tall, piece_next = (lax.axis_size("tp"), lax.axis_index("tp"), payload.shape[0])
+        w2 = vec_out = payload
+        part_now = lax.dynamic_update_slice_in_dim(
+            jnp.zeros(
+                [ii * then if nth == 0 else ii for nth, ii in enumerate(payload.shape)],
+                payload.dtype,
+            ),
+            payload,
+            tall * piece_next,
+            axis=0,
+        )
+        for k0 in range(1, then // 2 + 1):
+            w2 = lax.ppermute(w2, "tp", list(map(lambda nth: (nth, (nth + 1) % then), range(then))))
+            part_now = lax.dynamic_update_slice_in_dim(
+                part_now, w2, (tall - k0) % then * piece_next, axis=0
+            )
+            if 2 * k0 < then:
+                vec_out = lax.ppermute(
+                    vec_out, "tp", list(map(lambda nth: (nth, (nth - 1) % then), range(then)))
+                )
+                part_now = lax.dynamic_update_slice_in_dim(
+                    part_now, vec_out, (tall + k0) % then * piece_next, axis=0
+                )
+        return part_now
+
+    rows_in = threads_lay(row_block)
     gate_value = jnp.dot(rows_in, gate_weight[0], preferred_element_type=jnp.float32)
     up_value = jnp.dot(rows_in, up_weight[0], preferred_element_type=jnp.float32)
     hidden = (jax.nn.silu(gate_value) * up_value).astype(jnp.bfloat16)

time: 336 us -> 357 us (1.062)
  starting transfers between devices: 22.1 us -> 42.6 us
    ppermute x0 -> x15, waiting for transfers between devices: none -> 45.2 us  [the longest x8 45.1 us: threads_lay(): lax.ppermute(w2, 'tp', list(map(lambda nth: (nth, (nth + 1) % then), rang...]
    all_gather x1 -> x0, waiting for transfers between devices: 40 us -> none  [shards(): rows_in = lax.all_gather(row_block, 'tp', axis=0, tiled=True)]
    ppermute x0 -> x15, starting transfers between devices: none -> 20.7 us  [the longest x7 20.7 us: threads_lay(): lax.ppermute(vec_out, 'tp', list(map(lambda nth: (nth, (nth - 1) % then),...]
    reduce_scatter x1, waiting for transfers between devices: 65.9 us -> 61.2 us  [shards(): lax.psum_scatter(jnp.dot(hidden, down_weight[0], preferred_element_type=j...]
    unnamed x17 -> x21, local copies, waits for them, and re-layouts: 9.73 us -> 12.4 us
  transfers between devices with their start and end apart: 7 -> 21, of which waited for: 6 -> 13; matrix products, arithmetic and copies ran while one was open for 8% -> 8% of each run, Pallas kernels for 0% -> 0%
where the time goes in v1:
time: 357 us; the launch traced here: 356 us
  waiting for transfers between devices  188 us (53%)
  blocking collectives  44.9 us (13%)
  starting transfers between devices  42.6 us (12%)
  local copies, waits for them, and re-layouts  30.3 us (8%)
  matrix products  26.1 us (7%)
  between operations  13.5 us (4%)
  loops' own time  5.68 us (2%)
  other arithmetic  5.62 us (2%)
    reduce_scatter x1, waiting for transfers between devices, shards(): lax.psum_scatter(jnp.dot(hidden, down_weight[0], preferred_element_type=j...  61.2 us
    all_gather x1, waiting for transfers between devices, sent_together(): filled = lax.all_gather(both, axis, axis=dim, tiled=True)  49.1 us
    ppermute x8, waiting for transfers between devices, threads_lay(): lax.ppermute(w2, 'tp', list(map(lambda nth: (nth, (nth + 1) % then), rang...  45.1 us
    all_to_all x1, blocking collectives, shards(): lax.all_to_all(dispatch, 'sp', split_axis=0, concat_axis=0, tiled=True)  44.9 us
    ppermute x7, starting transfers between devices, threads_lay(): lax.ppermute(vec_out, 'tp', list(map(lambda nth: (nth, (nth - 1) % then),...  20.7 us
    dot_general x1, matrix products, shards(): jnp.dot(hidden, down_weight[0], preferred_element_type=jnp.float32)  13.2 us
    all_gather x1, waiting for transfers between devices, shards(): lax.all_gather(out_weight, 'tp', axis=0, tiled=True)  12.6 us
    unnamed x21, local copies, waits for them, and re-layouts  12.4 us
  transfers between devices with their start and end apart: 21, of which 13 were waited for; matrix products, arithmetic and copies ran while one was open for 8% of the time, Pallas kernels for 0%

profile of v1, /device:TPU:2, one launch (start us, length us, event | category | flops | bytes accessed | tf_op | source)
XLA Modules:
  0.0 356.4 jit_solution(4255688769475281938)
XLA Ops:
  6.5 1.8 pad_maximum_fusion
  8.5 0.7 all-gather.5.cloned.1.call-update
  9.2 1.3 broadcast_in_dim.64
  10.5 7.5 %all-to-all-start = ((f32[16,512,2]{1,2,0:T(2,128)}), f32[16,512,2]{1,2,0:T(2,128)S(1)}, u32[]{:S(2)}, u32[]{:S(2)}) async-start(f32[16,512,2]{1,2,0:T(2,128)} %broadcast_in_dim.64), calls=%async_computation | async-start | bytes 131072 | tf_op jit(solution)/shard_map/all_to_all | solution.py:12
  18.0 1.0 copy.28
  19.0 0.8 copy.33
  20.0 49.1 %all-gather.3.cloned.1.call-done = bf16[8192,256]{1,0:T(8,128)(2,1)} async-done(((bf16[512,256]{1,0:T(8,128)(2,1)}), bf16[8192,256]{1,0:T(8,128)(2,1)}) %all-gather.3.cloned.1.call-update) | async-done | bytes 4194320 | tf_op jit(solution)/shard_map/all_gather | solution.py:31
  69.2 4.4 %fusion.32 = (bf16[8192,128]{1,0:T(8,128)(2,1)}, bf16[8192,128]{1,0:T(8,128)(2,1)}) fusion(bf16[8192,256]{1,0:T(8,128)(2,1)} %all-gather.3.cloned.1.call-done), kind=kLoop, calls=%fused_computation.70 | loop fusion | bytes 8388608 | tf_op jit(solution)/shard_map/split | solution.py:32
  73.6 4.0 %copy.29 = bf16[8,1024,128]{1,2,0:T(8,128)(2,1)} copy(bf16[8,1024,128]{2,1,0:T(8,128)(2,1)} %bitcast.62) | data formatting | bytes 4194304
  77.6 3.9 %copy.30 = bf16[8,1024,128]{1,2,0:T(8,128)(2,1)} copy(bf16[8,1024,128]{2,1,0:T(8,128)(2,1)} %bitcast.61) | data formatting | bytes 4194304
  81.6 16.5 %while.15 = (s32[]{:T(128)}, f32[2,512]{1,0:T(2,128)S(1)}, f32[2,512]{1,0:T(2,128)S(1)}, f32[2,512,64]{1,2,0:T(8,128)S(1)}, s32[8]{0:T(128)S(1)}, /*index=5*/s32...) while((s32[]{:T(128)}, f32[2,512]{1,0:T(2,128)S(1)}, ...), condition=%wide.region_5.6_spmd.clone, body=%wide.region_0.5_spmd.clone.sunk | while | flops 289017344 | bytes 17043828 | solution.py:113
  82.8 6.2 %conditional.3 = ((f32[2,512]{1,0:T(2,128)S(1)}, f32[2,512]{1,0:T(2,128)S(1)}, f32[2,512,64]{1,2,0:T(8,128)S(1)})) conditional(s32[]{:T(128)} %convert_element_type.83, (f32[2,512]{1,0:T(2,128)S(1)}, f32[2,512]{1,0:T(2,128)S(1)}, f32[2,512,64]{1,2,0:T(8,128)S(1)}) %tuple.43, (s32[]{:T(128)}, s32[]{:T(128)}, bf16[8,1024,128]{1,2,0:T(8,128)(2,1)}, ...), branch_computations={%region_1.1_spmd, %region_2.4_spmd} | conditional | flops 289017344 | bytes 17041490 | solution.py:111
  83.3 1.1 constant_dynamic-slice_fusion
  84.4 1.4 fusion.4
  85.8 1.5 fusion.3
  87.3 1.7 fusion.8
  98.3 0.8 all_to_all.24
  99.1 7.1 %all-to-all-start.1 = ((bf16[16,32,128]{2,1,0:T(8,128)(2,1)}), bf16[16,32,128]{2,1,0:T(8,128)(2,1)S(1)}, u32[]{:S(2)}, u32[]{:S(2)}) async-start(bf16[16,32,128]{2,1,0:T(8,128)(2,1)} %all_to_all.24), calls=%async_computation.1 | async-start | bytes 262144 | tf_op jit(solution)/shard_map/all_to_all | solution.py:121
  106.4 10.3 %all-to-all-done.1 = bf16[16,32,128]{2,1,0:T(8,128)(2,1)S(1)} async-done(((bf16[16,32,128]{2,1,0:T(8,128)(2,1)}), bf16[16,32,128]{2,1,0:T(8,128)(2,1)S(1)}, u32[]{:S(2)}, u32[]{:S(2)}) %all-to-all-start.1) | async-done | bytes 131104 | tf_op jit(solution)/shard_map/all_to_all | solution.py:121
  116.8 12.6 %all-gather.5.cloned.1.call-done = bf16[2048,2048]{1,0:T(8,128)(2,1)} async-done(((bf16[128,2048]{1,0:T(8,128)(2,1)}), bf16[2048,2048]{1,0:T(8,128)(2,1)}) %all-gather.5.cloned.1.call-update) | async-done | bytes 8388624 | tf_op jit(solution)/shard_map/all_gather | solution.py:124
  129.4 5.0 %multiply_reduce_fusion.1 = (f32[32]{0:T(128)S(1)}, f32[32,2048]{1,0:T(8,128)S(1)}) fusion(bf16[2048,2048]{1,0:T(8,128)(2,1)} %all-gather.5.cloned.1.call-done, bf16[32,2048]{1,0:T(8,128)(2,1)S(1)} %copy-done.3, bf16[16,32,128]{2,1,0:T(8,128)(2,1)S(1)} %all-to-all-done.1), kind=kOutput, calls=%fused_computation.36 | convolution fusion | flops 268828640 | bytes 8913024 | tf_op jit(solution)/shard_map/dot_general | solution.py:122
  135.2 44.9 %all_to_all.34 = bf16[16,6,2048]{2,1,0:T(8,128)(2,1)S(1)} all-to-all(bf16[16,6,2048]{2,1,0:T(8,128)(2,1)S(1)} %reshape.145), channel_id=1, replica_groups=mesh['sp'=16,'tp'=16] {'sp'}, dimensions={0} | all-to-all | bytes 786432 | tf_op jit(solution)/shard_map/all_to_all | solution.py:145
  180.3 2.9 collective-permute-start.1
  183.2 0.8 broadcast_in_dim.65
  184.1 4.6 %collective-permute-done = bf16[96,2048]{1,0:T(8,128)(2,1)S(1)} collective-permute-done((bf16[96,2048]{1,0:T(8,128)(2,1)S(1)}, bf16[96,2048]{1,0:T(8,128)(2,1)S(1)}, u32[]{:S(2)}, u32[]{:S(2)}) %collective-permute-start) | collective-permute-done | bytes 393248 | tf_op jit(solution)/shard_map/ppermute | solution.py:161
  188.7 3.0 collective-permute-start.3
  191.8 5.4 %collective-permute-done.2 = bf16[96,2048]{1,0:T(8,128)(2,1)S(1)} collective-permute-done((bf16[96,2048]{1,0:T(8,128)(2,1)S(1)}, bf16[96,2048]{1,0:T(8,128)(2,1)S(1)}, u32[]{:S(2)}, u32[]{:S(2)}) %collective-permute-start.2) | collective-permute-done | bytes 393248 | tf_op jit(solution)/shard_map/ppermute | solution.py:161
  197.1 3.0 collective-permute-start.5
  200.2 5.4 %collective-permute-done.4 = bf16[96,2048]{1,0:T(8,128)(2,1)S(1)} collective-permute-done((bf16[96,2048]{1,0:T(8,128)(2,1)S(1)}, bf16[96,2048]{1,0:T(8,128)(2,1)S(1)}, u32[]{:S(2)}, u32[]{:S(2)}) %collective-permute-start.4) | collective-permute-done | bytes 393248 | tf_op jit(solution)/shard_map/ppermute | solution.py:161
  205.5 3.0 collective-permute-start.7
  208.6 5.4 %collective-permute-done.6 = bf16[96,2048]{1,0:T(8,128)(2,1)S(1)} collective-permute-done((bf16[96,2048]{1,0:T(8,128)(2,1)S(1)}, bf16[96,2048]{1,0:T(8,128)(2,1)S(1)}, u32[]{:S(2)}, u32[]{:S(2)}) %collective-permute-start.6) | collective-permute-done | bytes 393248 | tf_op jit(solution)/shard_map/ppermute | solution.py:161
  213.9 3.0 collective-permute-start.9
  217.0 5.4 %collective-permute-done.8 = bf16[96,2048]{1,0:T(8,128)(2,1)S(1)} collective-permute-done((bf16[96,2048]{1,0:T(8,128)(2,1)S(1)}, bf16[96,2048]{1,0:T(8,128)(2,1)S(1)}, u32[]{:S(2)}, u32[]{:S(2)}) %collective-permute-start.8) | collective-permute-done | bytes 393248 | tf_op jit(solution)/shard_map/ppermute | solution.py:161
  222.4 3.0 collective-permute-start.11
  225.4 5.4 %collective-permute-done.10 = bf16[96,2048]{1,0:T(8,128)(2,1)S(1)} collective-permute-done((bf16[96,2048]{1,0:T(8,128)(2,1)S(1)}, bf16[96,2048]{1,0:T(8,128)(2,1)S(1)}, u32[]{:S(2)}, u32[]{:S(2)}) %collective-permute-start.10) | collective-permute-done | bytes 393248 | tf_op jit(solution)/shard_map/ppermute | solution.py:161
  230.8 3.0 collective-permute-start.13
  233.8 5.4 %collective-permute-done.12 = bf16[96,2048]{1,0:T(8,128)(2,1)S(1)} collective-permute-done((bf16[96,2048]{1,0:T(8,128)(2,1)S(1)}, bf16[96,2048]{1,0:T(8,128)(2,1)S(1)}, u32[]{:S(2)}, u32[]{:S(2)}) %collective-permute-start.12) | collective-permute-done | bytes 393248 | tf_op jit(solution)/shard_map/ppermute | solution.py:161
  239.3 8.3 %collective-permute-done.14 = bf16[96,2048]{1,0:T(8,128)(2,1)S(1)} collective-permute-done((bf16[96,2048]{1,0:T(8,128)(2,1)S(1)}, bf16[96,2048]{1,0:T(8,128)(2,1)S(1)}, u32[]{:S(2)}, u32[]{:S(2)}) %collective-permute-start.14) | collective-permute-done | bytes 393248 | tf_op jit(solution)/shard_map/ppermute | solution.py:161
  247.6 2.6 copy-done.1
  250.2 4.6 %fusion.21 = f32[1536,448]{0,1:T(8,128)} fusion(bf16[1536,2048]{1,0:T(8,128)(2,1)S(1)} %constant_dynamic-update-slice_fusion, bf16[1,2048,448]{1,2,0:T(8,128)(2,1)S(1)} %copy-done.7), kind=kOutput, calls=%fused_computation.30 | convolution fusion | flops 2818572288 | bytes 10878976 | tf_op jit(solution)/shard_map/dot_general | solution.py:175
  254.8 13.2 %convolution_convert_fusion = bf16[1536,2048]{1,0:T(8,128)(2,1)} fusion(bf16[1,448,2048]{2,1,0:T(8,128)(2,1)S(1)} %copy-done, f32[1536,448]{0,1:T(8,128)} %fusion.21, bf16[1536,2048]{1,0:T(8,128)(2,1)} %copy-done.1, bf16[1,2048,448]{1,2,0:T(8,128)(2,1)} %param.24), kind=kOutput, calls=%fused_computation.21 | convolution fusion | flops 5644419072 | bytes 19005440 | tf_op jit(solution)/shard_map/dot_general | solution.py:179
  268.1 61.2 %reduce-scatter.2.cloned.1.call-done = bf16[96,2048]{1,0:T(8,128)(2,1)} async-done(((bf16[1536,2048]{1,0:T(8,128)(2,1)}), bf16[96,2048]{1,0:T(8,128)(2,1)}) %reduce-scatter.2.cloned.1.call-update) | async-done | bytes 393232 | tf_op jit(solution)/shard_map/reduce_scatter | solution.py:178
  329.3 1.9 reshape.147
  331.2 7.3 %all-to-all-start.3 = ((bf16[16,6,2048]{2,1,0:T(8,128)(2,1)}), bf16[16,6,2048]{2,1,0:T(8,128)(2,1)S(1)}, u32[]{:S(2)}, u32[]{:S(2)}) async-start(bf16[16,6,2048]{2,1,0:T(8,128)(2,1)} %reshape.147), calls=%async_computation.4 | async-start | bytes 1048576 | tf_op jit(solution)/shard_map/all_to_all | solution.py:185
  338.8 8.5 %all-to-all-done.3 = bf16[16,6,2048]{2,1,0:T(8,128)(2,1)S(1)} async-done(((bf16[16,6,2048]{2,1,0:T(8,128)(2,1)}), bf16[16,6,2048]{2,1,0:T(8,128)(2,1)S(1)}, u32[]{:S(2)}, u32[]{:S(2)}) %all-to-all-start.3) | async-done | bytes 393248 | tf_op jit(solution)/shard_map/all_to_all | solution.py:185
  347.4 0.7 gather_fusion
  348.5 0.7 multiply_reduce_fusion
  349.2 0.7 add_convert_fusion
  (108 shorter events, 8.3 us)
Async XLA Ops:
  6.5 248.3 %copy-start = (bf16[1,448,2048]{2,1,0:T(8,128)(2,1)S(1)}, bf16[1,448,2048]{2,1,0:T(8,128)(2,1)}, u32[]{:S(2)}) copy-start(bf16[1,448,2048]{2,1,0:T(8,128)(2,1)} %param.25) | copy-start | bytes 5505028
  6.5 62.6 %all-gather.3.cloned.1.call-start = ((), (), s32[]{:S(2)}) async-start(), calls=%async_computation.5 | async-start | bytes 4456448 | tf_op jit(solution)/shard_map/all_gather | solution.py:31
  8.4 121.0 %all-gather.5.cloned.1.call-start = ((), (), s32[]{:S(2)}) async-start(), calls=%async_computation.6 | async-start | bytes 8912896 | tf_op jit(solution)/shard_map/all_gather | solution.py:124
  10.5 71.0 %all-to-all-start = ((f32[16,512,2]{1,2,0:T(2,128)}), f32[16,512,2]{1,2,0:T(2,128)S(1)}, u32[]{:S(2)}, u32[]{:S(2)}) async-start(f32[16,512,2]{1,2,0:T(2,128)} %broadcast_in_dim.64), calls=%async_computation | async-start | bytes 131072 | tf_op jit(solution)/shard_map/all_to_all | solution.py:12
  73.6 7.9 %copy-start.2 = (f32[512,2]{0,1:T(2,128)S(1)}, f32[512,2]{0,1:T(2,128)}, u32[]{:S(2)}) copy-start(f32[512,2]{0,1:T(2,128)} %param.20) | copy-start | bytes 12292
  81.5 47.9 %copy-start.3 = (bf16[32,2048]{1,0:T(8,128)(2,1)S(1)}, bf16[32,2048]{1,0:T(8,128)(2,1)}, u32[]{:S(2)}) copy-start(bf16[32,2048]{1,0:T(8,128)(2,1)} %param.16) | copy-start | bytes 393220
  99.1 17.7 %all-to-all-start.1 = ((bf16[16,32,128]{2,1,0:T(8,128)(2,1)}), bf16[16,32,128]{2,1,0:T(8,128)(2,1)S(1)}, u32[]{:S(2)}, u32[]{:S(2)}) async-start(bf16[16,32,128]{2,1,0:T(8,128)(2,1)} %all_to_all.24), calls=%async_computation.1 | async-start | bytes 262144 | tf_op jit(solution)/shard_map/all_to_all | solution.py:121
  106.2 223.1 %reduce-scatter.2.cloned.1.call-start = ((), (), s32[]{:S(2)}) async-start(), calls=%async_computation.7 | async-start | bytes 6684672 | tf_op jit(solution)/shard_map/reduce_scatter | solution.py:178
  106.4 28.0 %copy-start.4 = (f32[2048]{0:T(1024)S(1)}, f32[2048]{0:T(1024)}, u32[]{:S(2)}) copy-start(f32[2048]{0:T(1024)} %param.22) | copy-start | bytes 24580
  180.3 8.4 %collective-permute-start = (bf16[96,2048]{1,0:T(8,128)(2,1)S(1)}, bf16[96,2048]{1,0:T(8,128)(2,1)S(1)}, u32[]{:S(2)}, u32[]{:S(2)}) collective-permute-start(bf16[96,2048]{1,0:T(8,128)(2,1)S(1)} %reshape.146), channel_id=1, source_target_pairs={{0,1},{1,2},{2,3},{3,4},{4,5},{5,6},{6,7},{7,8},{8,9},{9,10},{10,1... | collective-permute-start | bytes 1179656 | tf_op jit(solution)/shard_map/ppermute | solution.py:161
  180.3 8.4 %collective-permute-start.1 = (bf16[96,2048]{1,0:T(8,128)(2,1)S(1)}, bf16[96,2048]{1,0:T(8,128)(2,1)S(1)}, u32[]{:S(2)}, u32[]{:S(2)}) collective-permute-start(bf16[96,2048]{1,0:T(8,128)(2,1)S(1)} %reshape.146), channel_id=1, source_target_pairs={{0,15},{1,0},{2,1},{3,2},{4,3},{5,4},{6,5},{7,6},{8,7},{9,8},{10,9... | collective-permute-start | bytes 1179656 | tf_op jit(solution)/shard_map/ppermute | solution.py:166
  188.7 8.4 %collective-permute-start.2 = (bf16[96,2048]{1,0:T(8,128)(2,1)S(1)}, bf16[96,2048]{1,0:T(8,128)(2,1)S(1)}, u32[]{:S(2)}, u32[]{:S(2)}) collective-permute-start(bf16[96,2048]{1,0:T(8,128)(2,1)S(1)} %collective-permute-done), channel_id=1, source_target_pairs={{0,1},{1,2},{2,3},{3,4},{4,5},{5,6},{6,7},{7,8},{8,9},{9,10},{10,1... | collective-permute-start | bytes 1179656 | tf_op jit(solution)/shard_map/ppermute | solution.py:161
  188.7 8.4 %collective-permute-start.3 = (bf16[96,2048]{1,0:T(8,128)(2,1)S(1)}, bf16[96,2048]{1,0:T(8,128)(2,1)S(1)}, u32[]{:S(2)}, u32[]{:S(2)}) collective-permute-start(bf16[96,2048]{1,0:T(8,128)(2,1)S(1)} %collective-permute-done.1), channel_id=1, source_target_pairs={{0,15},{1,0},{2,1},{3,2},{4,3},{5,4},{6,5},{7,6},{8,7},{9,8},{10,9... | collective-permute-start | bytes 1179656 | tf_op jit(solution)/shard_map/ppermute | solution.py:166
  197.1 8.4 %collective-permute-start.4 = (bf16[96,2048]{1,0:T(8,128)(2,1)S(1)}, bf16[96,2048]{1,0:T(8,128)(2,1)S(1)}, u32[]{:S(2)}, u32[]{:S(2)}) collective-permute-start(bf16[96,2048]{1,0:T(8,128)(2,1)S(1)} %collective-permute-done.2), channel_id=1, source_target_pairs={{0,1},{1,2},{2,3},{3,4},{4,5},{5,6},{6,7},{7,8},{8,9},{9,10},{10,1... | collective-permute-start | bytes 1179656 | tf_op jit(solution)/shard_map/ppermute | solution.py:161
  197.1 8.4 %collective-permute-start.5 = (bf16[96,2048]{1,0:T(8,128)(2,1)S(1)}, bf16[96,2048]{1,0:T(8,128)(2,1)S(1)}, u32[]{:S(2)}, u32[]{:S(2)}) collective-permute-start(bf16[96,2048]{1,0:T(8,128)(2,1)S(1)} %collective-permute-done.3), channel_id=1, source_target_pairs={{0,15},{1,0},{2,1},{3,2},{4,3},{5,4},{6,5},{7,6},{8,7},{9,8},{10,9... | collective-permute-start | bytes 1179656 | tf_op jit(solution)/shard_map/ppermute | solution.py:166
  200.2 50.1 %copy-start.7 = (bf16[1,2048,448]{1,2,0:T(8,128)(2,1)S(1)}, bf16[1,2048,448]{1,2,0:T(8,128)(2,1)}, u32[]{:S(2)}) copy-start(bf16[1,2048,448]{1,2,0:T(8,128)(2,1)} %param.23) | copy-start | bytes 5505028
  205.5 8.4 %collective-permute-start.6 = (bf16[96,2048]{1,0:T(8,128)(2,1)S(1)}, bf16[96,2048]{1,0:T(8,128)(2,1)S(1)}, u32[]{:S(2)}, u32[]{:S(2)}) collective-permute-start(bf16[96,2048]{1,0:T(8,128)(2,1)S(1)} %collective-permute-done.4), channel_id=1, source_target_pairs={{0,1},{1,2},{2,3},{3,4},{4,5},{5,6},{6,7},{7,8},{8,9},{9,10},{10,1... | collective-permute-start | bytes 1179656 | tf_op jit(solution)/shard_map/ppermute | solution.py:161
  205.5 8.4 %collective-permute-start.7 = (bf16[96,2048]{1,0:T(8,128)(2,1)S(1)}, bf16[96,2048]{1,0:T(8,128)(2,1)S(1)}, u32[]{:S(2)}, u32[]{:S(2)}) collective-permute-start(bf16[96,2048]{1,0:T(8,128)(2,1)S(1)} %collective-permute-done.5), channel_id=1, source_target_pairs={{0,15},{1,0},{2,1},{3,2},{4,3},{5,4},{6,5},{7,6},{8,7},{9,8},{10,9... | collective-permute-start | bytes 1179656 | tf_op jit(solution)/shard_map/ppermute | solution.py:166
  213.9 8.4 %collective-permute-start.8 = (bf16[96,2048]{1,0:T(8,128)(2,1)S(1)}, bf16[96,2048]{1,0:T(8,128)(2,1)S(1)}, u32[]{:S(2)}, u32[]{:S(2)}) collective-permute-start(bf16[96,2048]{1,0:T(8,128)(2,1)S(1)} %collective-permute-done.6), channel_id=1, source_target_pairs={{0,1},{1,2},{2,3},{3,4},{4,5},{5,6},{6,7},{7,8},{8,9},{9,10},{10,1... | collective-permute-start | bytes 1179656 | tf_op jit(solution)/shard_map/ppermute | solution.py:161
  213.9 8.4 %collective-permute-start.9 = (bf16[96,2048]{1,0:T(8,128)(2,1)S(1)}, bf16[96,2048]{1,0:T(8,128)(2,1)S(1)}, u32[]{:S(2)}, u32[]{:S(2)}) collective-permute-start(bf16[96,2048]{1,0:T(8,128)(2,1)S(1)} %collective-permute-done.7), channel_id=1, source_target_pairs={{0,15},{1,0},{2,1},{3,2},{4,3},{5,4},{6,5},{7,6},{8,7},{9,8},{10,9... | collective-permute-start | bytes 1179656 | tf_op jit(solution)/shard_map/ppermute | solution.py:166
  222.4 8.4 %collective-permute-start.10 = (bf16[96,2048]{1,0:T(8,128)(2,1)S(1)}, bf16[96,2048]{1,0:T(8,128)(2,1)S(1)}, u32[]{:S(2)}, u32[]{:S(2)}) collective-permute-start(bf16[96,2048]{1,0:T(8,128)(2,1)S(1)} %collective-permute-done.8), channel_id=1, source_target_pairs={{0,1},{1,2},{2,3},{3,4},{4,5},{5,6},{6,7},{7,8},{8,9},{9,10},{10,1... | collective-permute-start | bytes 1179656 | tf_op jit(solution)/shard_map/ppermute | solution.py:161
  222.4 8.4 %collective-permute-start.11 = (bf16[96,2048]{1,0:T(8,128)(2,1)S(1)}, bf16[96,2048]{1,0:T(8,128)(2,1)S(1)}, u32[]{:S(2)}, u32[]{:S(2)}) collective-permute-start(bf16[96,2048]{1,0:T(8,128)(2,1)S(1)} %collective-permute-done.9), channel_id=1, source_target_pairs={{0,15},{1,0},{2,1},{3,2},{4,3},{5,4},{6,5},{7,6},{8,7},{9,8},{10,9... | collective-permute-start | bytes 1179656 | tf_op jit(solution)/shard_map/ppermute | solution.py:166
  230.8 8.4 %collective-permute-start.12 = (bf16[96,2048]{1,0:T(8,128)(2,1)S(1)}, bf16[96,2048]{1,0:T(8,128)(2,1)S(1)}, u32[]{:S(2)}, u32[]{:S(2)}) collective-permute-start(bf16[96,2048]{1,0:T(8,128)(2,1)S(1)} %collective-permute-done.10), channel_id=1, source_target_pairs={{0,1},{1,2},{2,3},{3,4},{4,5},{5,6},{6,7},{7,8},{8,9},{9,10},{10,1... | collective-permute-start | bytes 1179656 | tf_op jit(solution)/shard_map/ppermute | solution.py:161
  230.8 8.5 %collective-permute-start.13 = (bf16[96,2048]{1,0:T(8,128)(2,1)S(1)}, bf16[96,2048]{1,0:T(8,128)(2,1)S(1)}, u32[]{:S(2)}, u32[]{:S(2)}) collective-permute-start(bf16[96,2048]{1,0:T(8,128)(2,1)S(1)} %collective-permute-done.11), channel_id=1, source_target_pairs={{0,15},{1,0},{2,1},{3,2},{4,3},{5,4},{6,5},{7,6},{8,7},{9,8},{10,9... | collective-permute-start | bytes 1179656 | tf_op jit(solution)/shard_map/ppermute | solution.py:166
  239.2 8.4 %collective-permute-start.14 = (bf16[96,2048]{1,0:T(8,128)(2,1)S(1)}, bf16[96,2048]{1,0:T(8,128)(2,1)S(1)}, u32[]{:S(2)}, u32[]{:S(2)}) collective-permute-start(bf16[96,2048]{1,0:T(8,128)(2,1)S(1)} %collective-permute-done.12), channel_id=1, source_target_pairs={{0,1},{1,2},{2,3},{3,4},{4,5},{5,6},{6,7},{7,8},{8,9},{9,10},{10,1... | collective-permute-start | bytes 1179656 | tf_op jit(solution)/shard_map/ppermute | solution.py:161
  247.6 2.6 copy-start.1
  268.0 70.5 %copy-start.5 = (s32[32,2]{0,1:T(2,128)S(1)}, s32[32,2]{0,1:T(2,128)}, u32[]{:S(2)}) copy-start(s32[32,2]{0,1:T(2,128)} %param.26) | copy-start | bytes 772
  268.0 70.7 %copy-start.6 = (f32[32,2]{0,1:T(2,128)S(1)}, f32[32,2]{0,1:T(2,128)}, u32[]{:S(2)}) copy-start(f32[32,2]{0,1:T(2,128)} %param.27) | copy-start | bytes 772
  331.2 16.0 %all-to-all-start.3 = ((bf16[16,6,2048]{2,1,0:T(8,128)(2,1)}), bf16[16,6,2048]{2,1,0:T(8,128)(2,1)S(1)}, u32[]{:S(2)}, u32[]{:S(2)}) async-start(bf16[16,6,2048]{2,1,0:T(8,128)(2,1)} %reshape.147), calls=%async_computation.4 | async-start | bytes 1048576 | tf_op jit(solution)/shard_map/all_to_all | solution.py:185
Sparse Core Ops, SparseCore 0:
  9.8 59.3 all-gather.2
  71.0 58.3 all-gather.4
  268.2 61.0 reduce-scatter.1
